TPU v7x, 32 devices: a whole 2x2x4 slice. The times are simulated.
32 devices in a mesh: kv: 8 (over z, y), tp: 4 (over x, core).
Axes of the slice: x: 2, y: 2, z: 4, core: 2. Of those that a mesh axis runs over, the one named last changes fastest.
Arguments:
- tokens: bfloat16 [16, 4096], P(None, 'kv'), may hold values from -6 to 6
- norm_gain: float32 [4096], P('kv'), may hold values from 0.1 to 1.9
- query_weight: bfloat16 [4096, 2048], P('kv', 'tp'), may hold values from -1 to 1
- key_weight: bfloat16 [4096, 2048], P('kv', 'tp'), may hold values from -0.09375 to 0.09375
- value_weight: bfloat16 [4096, 2048], P('kv', 'tp'), may hold values from -0.09375 to 0.09375
- out_weight: bfloat16 [2048, 4096], P('tp', 'kv'), may hold values from -0.125 to 0.125
- lambdas: float32 [16], P('tp'), may hold values from 0.3 to 0.8
- head_gain: float32 [128], replicated, may hold values from 0.1 to 1.9
- lengths: int32 [16], replicated, may hold values from 1 to 8191, as said below
- key_cache: bfloat16 [16, 8192, 16, 128], P(None, 'kv', 'tp'), may hold values from -48 to 48, as said below
- value_cache: bfloat16 [16, 8192, 16, 128], P(None, 'kv', 'tp'), may hold values from -6 to 6
Outputs:
- attended: bfloat16 [16, 4096], P(None, 'kv')
Inputs may be any that keep to these rules, and one draw needn't show every extreme that they name: `lengths`: each sequence has 1 to 8191 cached tokens. `key_cache`: cached keys lie between -48 and 48.
All inputs are finite; a program needn't handle non-finite values.
Results may differ from a plain program's by a relative error of at most 0.012.
The roundings to bfloat16 on the way count: a program that leaves them out, or rounds other values in their place, can miss the bound.
Values may be sent and summed in bfloat16 or wider, within the bound.
A program may use at most 128 MiB of HBM per device.

v0:
```python
import jax
import jax.numpy as jnp
from jax import lax
from jax.sharding import PartitionSpec as P

D = 4096
DH = 64


epsilon = 1e-05
theta_base = 500000.0
floor_value = -1e30


def combined_all(value, axis, join):
    pieces = jax.tree.map(lambda part: lax.all_gather(part, axis), value)
    head = jax.tree.map(lambda part: part[0], pieces)
    tail = jax.tree.map(lambda part: part[1:], pieces)
    so_far, _ = lax.scan(lambda so_far, section: (join(so_far, section), None), head, tail)
    return so_far


def angles_for(positions, width):
    halfway = width // 2
    frequency = theta_base ** (-jnp.arange(halfway, dtype=jnp.float32) / halfway)
    return positions.astype(jnp.float32)[:, None] * frequency[None, :]


def rotate(values_in, angles):
    halfway = values_in.shape[-1] // 2
    cosine = jnp.cos(angles)[:, None, None, :]
    sine_part = jnp.sin(angles)[:, None, None, :]
    former = values_in[..., :halfway]
    latter = values_in[..., halfway:]
    return jnp.concatenate(
        [former * cosine - latter * sine_part, latter * cosine + former * sine_part], axis=-1
    )


def finish(query_sum, key_sum, value_sum, square_sum, positions, heads_here):
    scaling = lax.rsqrt(square_sum / D + epsilon)[:, None]
    own_count = query_sum.shape[0]
    angles = angles_for(positions, DH)
    query = rotate((query_sum * scaling).reshape(own_count, heads_here, 2, DH), angles).astype(
        jnp.bfloat16
    )
    fresh_key = rotate((key_sum * scaling).reshape(own_count, heads_here, 2, DH), angles).astype(
        jnp.bfloat16
    )
    fresh_value = (value_sum * scaling).reshape(own_count, heads_here, 2 * DH).astype(jnp.bfloat16)
    return (query, fresh_key, fresh_value)


def combine(former, latter):
    highest = jnp.maximum(former[0], latter[0])
    former_scale = jnp.exp(former[0] - highest)
    latter_scale = jnp.exp(latter[0] - highest)
    return (
        highest,
        former[1] * former_scale + latter[1] * latter_scale,
        former[2] * former_scale[..., None] + latter[2] * latter_scale[..., None],
    )


def local(
    tokens,
    norm_gain,
    query_weight,
    key_weight,
    value_weight,
    out_weight,
    lambdas,
    head_gain,
    lengths,
    key_cache,
    value_cache,
):
    seq_count = tokens.shape[0]
    heads_here = query_weight.shape[1] // (2 * DH)
    widened = tokens.astype(jnp.float32)
    squares = jnp.sum(widened * widened, axis=1)
    normed = (widened * norm_gain[None, :]).astype(jnp.bfloat16)
    query_part = jnp.dot(normed, query_weight, preferred_element_type=jnp.float32)
    key_part = jnp.dot(normed, key_weight, preferred_element_type=jnp.float32)
    value_part = jnp.dot(normed, value_weight, preferred_element_type=jnp.float32)
    query_sum, key_sum, value_sum, square_sum = lax.psum(
        (query_part, key_part, value_part, squares), "kv"
    )
    query, fresh_key, fresh_value = finish(
        query_sum, key_sum, value_sum, square_sum, lengths, heads_here
    )
    pos_count = key_cache.shape[1]
    positions = lax.axis_index("kv") * pos_count + jnp.arange(pos_count, dtype=jnp.int32)
    key_blocks = key_cache.reshape(seq_count, pos_count, heads_here, 2, DH)
    scores = jnp.einsum(
        "shjd,sphjd->shjp", query, key_blocks, preferred_element_type=jnp.float32
    ) * DH ** (-0.5)
    fresh_score = jnp.einsum(
        "shjd,shjd->shj", query, fresh_key, preferred_element_type=jnp.float32
    ) * DH ** (-0.5)
    at_length = (positions[None, :] == lengths[:, None])[:, None, None, :]
    visible = (positions[None, :] <= lengths[:, None])[:, None, None, :]
    scores = jnp.where(at_length, fresh_score[..., None], scores)
    masked = jnp.where(visible, scores, floor_value)
    block_max = jnp.max(masked, axis=-1)
    weights = jnp.where(visible, jnp.exp(masked - block_max[..., None]), 0.0).astype(jnp.bfloat16)
    totals = jnp.sum(weights.astype(jnp.float32), axis=-1)
    cached_weights = jnp.where(at_length, jnp.zeros_like(weights), weights)
    weighted = jnp.einsum(
        "shjp,sphe->shje", cached_weights, value_cache, preferred_element_type=jnp.float32
    )
    fresh_weight = jnp.sum(
        jnp.where(at_length, weights, jnp.zeros_like(weights)).astype(jnp.float32), axis=-1
    )
    weighted = weighted + fresh_weight[..., None] * fresh_value[:, :, None, :].astype(jnp.float32)
    highest, totals, weighted = combined_all((block_max, totals, weighted), "kv", combine)
    mixed_heads = (
        weighted[:, :, 0] / totals[:, :, 0, None]
        - lambdas[None, :, None] * weighted[:, :, 1] / totals[:, :, 1, None]
    )
    head_out = (
        mixed_heads
        * lax.rsqrt(jnp.mean(mixed_heads * mixed_heads, axis=-1, keepdims=True) + epsilon)
        * head_gain
    )
    head_out = head_out.astype(jnp.bfloat16).reshape(seq_count, heads_here * 2 * DH)
    partial_value = jnp.dot(head_out, out_weight, preferred_element_type=jnp.float32)
    return lax.psum(partial_value, "tp").astype(jnp.bfloat16)


def solution(mesh):
    return jax.shard_map(
        local,
        mesh=mesh,
        in_specs=(
            P(None, "kv"),
            P("kv"),
            P("kv", "tp"),
            P("kv", "tp"),
            P("kv", "tp"),
            P("tp", "kv"),
            P("tp"),
            P(),
            P(),
            P(None, "kv", "tp", None),
            P(None, "kv", "tp", None),
        ),
        out_specs=P(None, "kv"),
        check_vma=False,
    )
```

profile of v0, /device:TPU:0, one launch (start us, length us, event | category | flops | bytes accessed | tf_op | source)
XLA Modules:
  0.0 224.9 jit_solution(2817768374999309295)
XLA Ops:
  6.5 1.5 fusion.17
  8.0 1.5 fusion.27
  9.5 1.9 fusion.29
  11.4 1.9 fusion.31
  13.3 0.7 convert_element_type.48
  13.9 0.7 broadcast_compare_fusion.1
  14.8 0.7 broadcast_bitcast_fusion
  15.6 26.2 %copy.33 = bf16[16,1024,4,128]{1,3,2,0:T(8,128)(2,1)} copy(bf16[16,1024,4,128]{3,2,1,0:T(4,128)(2,1)} %param.22) | data formatting | bytes 33554432 | tf_op args[9]
  41.8 44.6 %all-reduce.3.cloned.1.call-done = (f32[16,512]{1,0:T(8,128)}, f32[16]{0:T(128)}, f32[16,512]{1,0:T(8,128)}, f32[16,512]{1,0:T(8,128)}) async-done(((f32[16,512]{1,0:T(8,128)}, f32[16]{0:T(128)}, f32[16,512]{1,0:T(8,128)}, f32[16,512]{1,0:T(8,128)}), (f32[16,512]{1,0:T(8,128)}, f32[16]{0:T(128)}, f32[16,512]{1,0:T(8,128)}, f32[16,512]{1,0:T(8,128)})) %all-reduce.3.cloned.1.call-update) | async-done | bytes 98384 | tf_op jit(solution)/shard_map/psum | solution.py:86
  86.4 0.6 add_rsqrt_fusion.1
  87.0 0.9 fusion.22
  88.8 8.0 %fusion.13 = f32[16,4,2,1,1024]{4,3,2,1,0:T(1,128)S(1)} fusion(bf16[16,1024,4,2,64]{1,4,3,2,0:T(8,128)(2,1)} %bitcast.90, bf16[16,4,2,64,1]{3,2,1,0,4:T(2,128)(2,1)S(1)} %fusion.35), kind=kOutput, calls=%fused_computation.24 | convolution fusion | flops 16777216 | bytes 17317888 | tf_op jit(solution)/shard_map/shjd,sphjd->shjp/dot_general | solution.py:95
  96.8 0.9 fusion.33
  97.7 1.7 convert_reduce_fusion
  99.4 8.2 %fusion.6 = f32[16,4,2,128]{3,2,1,0:T(2,128)S(1)} fusion(bf16[16,1024,4,128]{3,2,1,0:T(4,128)(2,1)} %param.23, bf16[16,4,2,1024]{3,2,1,0:T(2,128)(2,1)S(1)} %get-tuple-element.83, pred[16,1024]{1,0:T(8,128)(4,1)S(1)} %get-tuple-element.93, f32[16,4,128]{2,1,0:T(4,128)S(1)} %reshape.147, f32[16,4,2]{2,1,0:T(4,128)S(1)} %get-tuple-element.59), kind=kOutput, calls=%fused_computation.12 | convolution fusion | flops 33718272 | bytes 17154560 | tf_op jit(solution)/shard_map/shjp,sphe->shje/dot_general | solution.py:109
  107.7 31.6 %all-gather.2 = f32[128,4,2,128]{3,1,2,0:T(4,128)S(1)} all-gather(f32[16,4,2,128]{3,1,2,0:T(4,128)S(1)} %copy.37), channel_id=4, replica_groups=mesh['kv'=8,'tp'=4] {'kv'}, dimensions={0}, use_global_device_ids=true | all-gather | bytes 589824 | tf_op jit(solution)/shard_map/all_gather | solution.py:16
  139.5 30.5 %all-gather.1 = f32[128,4,2]{1,2,0:T(2,128)S(1)} all-gather(f32[16,4,2]{1,2,0:T(2,128)S(1)} %copy.35), channel_id=3, replica_groups=mesh['kv'=8,'tp'=4] {'kv'}, dimensions={0}, use_global_device_ids=true | all-gather | bytes 4608 | tf_op jit(solution)/shard_map/all_gather | solution.py:16
  170.3 30.5 %all-gather = f32[128,4,2]{1,2,0:T(2,128)S(1)} all-gather(f32[16,4,2]{1,2,0:T(2,128)S(1)} %copy.34), channel_id=2, replica_groups=mesh['kv'=8,'tp'=4] {'kv'}, dimensions={0}, use_global_device_ids=true | all-gather | bytes 4608 | tf_op jit(solution)/shard_map/all_gather | solution.py:16
  201.3 4.8 %while.14 = (s32[]{:T(128)}, f32[16,4,2]{0,1,2:T(4,128)S(1)}, f32[16,4,2]{0,1,2:T(4,128)S(1)}, f32[16,4,2,128]{3,2,1,0:T(2,128)S(1)}, f32[7,16,4,2]{1,2,3,0:T(4,...) while((s32[]{:T(128)}, f32[16,4,2]{0,1,2:T(4,128)S(1)}, ...), condition=%wide.region_9.10_spmd, body=%wide.region_8.9_spmd.sunk | while | flops 49922 | bytes 334941 | solution.py:19
  201.6 0.4 fusion.45
  202.3 0.4 fusion.45
  203.0 0.4 fusion.45
  203.7 0.4 fusion.45
  207.2 10.9 %psum.39 = bf16[16,512]{1,0:T(8,128)(2,1)} all-reduce(f32[16,512]{1,0:T(8,128)S(1)} %fusion.23), channel_id=1, replica_groups=mesh['kv'=8,'tp'=4] {'tp'}, use_global_device_ids=true, to_apply=%region_11.12 | all-reduce | flops 8192 | bytes 49152 | tf_op jit(solution)/shard_map/psum | solution.py:128
  (75 shorter events, 6.0 us)
Async XLA Ops:
  6.5 1.5 copy-start
  6.5 79.9 %all-reduce.3.cloned.1.call-start = ((), (), s32[]{:S(2)}) async-start(), calls=%async_computation | async-start | bytes 197632 | tf_op jit(solution)/shard_map/psum | solution.py:86
  99.4 107.1 %copy-start.2 = (f32[4]{0:T(128)S(1)}, f32[4]{0:T(128)}, u32[]{:S(2)}) copy-start(f32[4]{0:T(128)} %param.19) | copy-start | bytes 52
  99.4 107.5 %copy-start.1 = (bf16[512,512]{1,0:T(8,128)(2,1)S(1)}, bf16[512,512]{1,0:T(8,128)(2,1)}, u32[]{:S(2)}) copy-start(bf16[512,512]{1,0:T(8,128)(2,1)} %param.18) | copy-start | bytes 1572868
Sparse Core Ops, SparseCore 0:
  13.4 72.9 all-reduce.2
where the time goes:
time: 226 us; the launch traced here: 225 us
  blocking collectives  103 us (46%)
  waiting for transfers between devices  44.7 us (20%)
  local copies, waits for them, and re-layouts  30.3 us (13%)
  matrix products  21.7 us (10%)
  between operations  13.6 us (6%)
  other arithmetic  11.1 us (5%)
    all_gather x3, blocking collectives, combined_all(): pieces = jax.tree.map(lambda part: lax.all_gather(part, axis), value)  92.6 us
    psum x1, waiting for transfers between devices, local(): lax.psum((query_part, key_part, value_part, squares), 'kv')  44.6 us
    unnamed x7, local copies, waits for them, and re-layouts  26.2 us
    psum x1, blocking collectives, local(): return lax.psum(partial_value, 'tp').astype(jnp.bfloat16)  10.9 us
    dot_general x1, matrix products, local(): jnp.einsum('shjp,sphe->shje', cached_weights, value_cache, preferred_elem...  8.24 us
    dot_general x1, matrix products, local(): jnp.einsum('shjd,sphjd->shjp', query, key_blocks, preferred_element_type=...  8.05 us
  transfers between devices with their start and end apart: 1, of which 1 were waited for; matrix products, arithmetic and copies ran while one was open for 13% of the time, Pallas kernels for 0%

commit v1 on v0

v1 whole, which is shorter than its diff:
```python
import functools

import jax
import jax.numpy as jnp
import numpy as np
from jax import lax
from jax.experimental import pallas as pl
from jax.experimental.pallas import tpu as pltpu
from jax.sharding import PartitionSpec as P

DH = 64
LANES = 128
ROWS = 16
CHUNK = 1024
epsilon = 1e-05
theta_base = 500000.0
floor_value = -1e30
MESH = pl.DeviceIdType.MESH


def kernel(
    n_kv, n_tp,
    tok_h, gain_h, qw_h, kw_h, vw_h, ow_h, lam_s, hg_h, len_s, freq_h, k_h, v_h,
    out_ref,
    tok, gain, wbuf, owbuf, hg, freq, kbuf, vbuf, ids,
    part, part_in, fresh, mine, mine_in, heads, shares,
    small_sem, w_sem, k_sem, v_sem,
    s1, r1, s2, r2, s3, r3, s4, r4, s5, r5,
):
    me = lax.axis_index("kv")
    tp = lax.axis_index("tp")
    seqs = tok.shape[0]
    spk = seqs // n_kv
    width = tok.shape[1]
    hh = wbuf.shape[2] // LANES
    model = width * n_kv
    npairs = seqs // 2
    cols = kbuf.shape[1]
    pos_count = cols // hh
    base = me * pos_count
    start_pair = lax.div((me + 1) * spk + 1, 2)

    small = [
        pltpu.make_async_copy(src, dst, small_sem.at[n])
        for n, (src, dst) in enumerate(((tok_h, tok), (gain_h, gain), (freq_h, freq), (hg_h, hg)))
    ]
    weights_in = [
        pltpu.make_async_copy(src, wbuf.at[n], w_sem.at[n])
        for n, src in enumerate((qw_h, kw_h, vw_h))
    ]
    out_weight_in = pltpu.make_async_copy(ow_h, owbuf, w_sem.at[3])
    for copy in small + weights_in:
        copy.start()

    def pair_of(step):
        return lax.rem(start_pair + step, npairs)

    def cache_copies(step):
        at = pl.ds(2 * pair_of(step), 2)
        return (
            pltpu.make_async_copy(k_h.at[at], kbuf.at[pl.ds(2 * step, 2)], k_sem.at[step]),
            pltpu.make_async_copy(v_h.at[at], vbuf.at[pl.ds(2 * step, 2)], v_sem.at[step]),
        )

    for step in range(npairs):
        for copy in cache_copies(step):
            copy.start()
        if step == npairs // 2:
            out_weight_in.start()

    def kv_peer(j):
        return {"kv": lax.rem(me + j, n_kv), "tp": tp}

    def tp_peer(j):
        return {"kv": me, "tp": lax.rem(tp + j, n_tp)}

    barrier = pltpu.get_barrier_semaphore()
    for j in range(1, n_kv):
        pl.semaphore_signal(barrier, inc=1, device_id=kv_peer(j), device_id_type=MESH)
    for j in range(1, n_tp):
        pl.semaphore_signal(barrier, inc=1, device_id=tp_peer(j), device_id_type=MESH)

    column = lax.broadcasted_iota(jnp.int32, (2 * hh, cols), 1)
    row = lax.broadcasted_iota(jnp.int32, (2 * hh, cols), 0)
    same = lax.rem(column, hh) == lax.rem(row, hh)
    ids[...] = jnp.where(same, lax.div(column, hh), 1 << 30)

    for copy in small:
        copy.wait()
    turns = [
        (jnp.cos(angle), jnp.sin(angle))
        for angle in (
            jnp.full((1, LANES), len_s[me * spk + n], jnp.int32).astype(jnp.float32) * freq[...]
            for n in range(spk)
        )
    ]
    widened = tok[...].astype(jnp.float32)
    squares = jnp.sum(widened * widened, axis=1, keepdims=True)
    normed = (widened * gain[...]).astype(jnp.bfloat16)
    part[pl.ds(3 * hh, seqs, stride=ROWS), :] = jnp.broadcast_to(squares, (seqs, LANES))
    for n in range(3 * hh + 1, ROWS):
        part[pl.ds(n, seqs, stride=ROWS), :] = jnp.zeros((seqs, LANES), jnp.float32)
    for n in range(3):
        weights_in[n].wait()
        product = jnp.dot(normed, wbuf[n], preferred_element_type=jnp.float32)
        for h in range(hh):
            part[pl.ds(n * hh + h, seqs, stride=ROWS), :] = product[:, h * LANES:(h + 1) * LANES]

    pl.semaphore_wait(barrier, n_kv - 1 + n_tp - 1)

    block = spk * ROWS
    own = pl.ds(pl.multiple_of(me * block, block), block)
    sends = []
    for j in range(1, n_kv):
        peer = lax.rem(me + j, n_kv)
        copy = pltpu.make_async_remote_copy(
            part.at[pl.ds(pl.multiple_of(peer * block, block), block)], part_in.at[j - 1],
            s1.at[j - 1], r1.at[j - 1], device_id=kv_peer(j), device_id_type=MESH,
        )
        copy.start()
        sends.append(copy)
    total = part[own, :]
    for copy, j in zip(sends, range(1, n_kv)):
        copy.wait_recv()
        total = total + part_in[j - 1]

    lane = lax.broadcasted_iota(jnp.int32, (2 * hh, LANES), 1)
    low_half = lax.rem(lane, DH) < DH // 2
    for n in range(spk):
        piece = total[n * ROWS:(n + 1) * ROWS]
        scaled = piece * lax.rsqrt(piece[3 * hh:3 * hh + 1] / model + epsilon)
        turned = scaled[:2 * hh]
        other = jnp.where(
            low_half,
            -pltpu.roll(turned, LANES - DH // 2, 1),
            pltpu.roll(turned, DH // 2, 1),
        )
        turned = turned * turns[n][0] + other * turns[n][1]
        fresh[pl.ds(pl.multiple_of(me * block + n * ROWS, ROWS), ROWS), :] = jnp.concatenate(
            [turned, scaled[2 * hh:]], axis=0
        ).astype(jnp.bfloat16)
    for j in range(1, n_kv):
        copy = pltpu.make_async_remote_copy(
            fresh.at[own], fresh.at[own], s2.at[j - 1], r2.at[j - 1],
            device_id=kv_peer(j), device_id_type=MESH,
        )
        copy.start()
        sends.append(copy)
    for j in range(1, n_kv):
        source = lax.rem(me + n_kv - j, n_kv)
        there = pl.ds(pl.multiple_of(source * block, block), block)
        pltpu.make_async_remote_copy(
            fresh.at[there], fresh.at[there], s2.at[j - 1], r2.at[j - 1],
            device_id=kv_peer(j), device_id_type=MESH,
        ).wait_recv()

    lane_q = lax.broadcasted_iota(jnp.int32, (hh, LANES), 1)
    map_masks = [(lane_q < DH).astype(jnp.float32), (lane_q >= DH).astype(jnp.float32)]
    wide = lax.broadcasted_iota(jnp.int32, (2 * hh, LANES), 1)
    chunk = min(CHUNK, cols)

    def send_partial(s):
        owner = lax.div(s, spk)
        slot = lax.rem(owner - me + n_kv, n_kv) - 1
        local = lax.rem(s, spk)
        return owner, pltpu.make_async_remote_copy(
            mine.at[s], mine_in.at[slot, local], s3.at[s], r3.at[slot, local],
            device_id={"kv": owner, "tp": tp}, device_id_type=MESH,
        )

    def attend(step, carry):
        for copy in cache_copies(step):
            copy.wait()
        pair = pair_of(step)
        queries, fresh_scores, fresh_values, reach = [], [], [], []
        for u in range(2):
            s = 2 * pair + u
            rows = fresh[pl.ds(pl.multiple_of(s * ROWS, ROWS), ROWS), :].astype(jnp.float32)
            query = rows[:hh] * DH ** (-0.5)
            query = jnp.concatenate([query * map_masks[0], query * map_masks[1]], axis=0)
            keys = jnp.concatenate([rows[hh:2 * hh]] * 2, axis=0)
            reach.append(len_s[s] - base)
            inside = jnp.full((2 * hh, 1), reach[u], jnp.int32)
            inside = (inside >= 0) & (inside < pos_count)
            score = jnp.sum(query * keys, axis=1, keepdims=True)
            fresh_scores.append(jnp.where(inside, score, floor_value))
            fresh_values.append(jnp.concatenate([rows[2 * hh:3 * hh]] * 2, axis=0))
            queries.append(query.astype(jnp.bfloat16))
        none = jnp.zeros_like(queries[0])
        left = jnp.concatenate(
            [
                jnp.concatenate([queries[0], none], axis=1),
                jnp.concatenate([none, queries[1]], axis=1),
            ],
            axis=0,
        )
        masked = [[], []]
        for c in range(0, cols, chunk):
            keys = jnp.concatenate(
                [kbuf[2 * step, c:c + chunk, :], kbuf[2 * step + 1, c:c + chunk, :]], axis=1
            )
            scores = lax.dot_general(
                left, keys, (((1,), (1,)), ((), ())), preferred_element_type=jnp.float32
            )
            for u in range(2):
                masked[u].append(
                    jnp.where(
                        ids[:, c:c + chunk] < reach[u],
                        scores[u * 2 * hh:(u + 1) * 2 * hh],
                        floor_value,
                    )
                )
        tops, safe = [], []
        for u in range(2):
            joint = functools.reduce(jnp.maximum, masked[u])
            top = jnp.maximum(jnp.max(joint, axis=1, keepdims=True), fresh_scores[u])
            tops.append(top)
            safe.append(jnp.maximum(top, floor_value * 0.1))
        values = jnp.zeros((4 * hh, 2 * LANES), jnp.float32)
        sums = [None, None]
        for n, c in enumerate(range(0, cols, chunk)):
            both = []
            for u in range(2):
                weight = jnp.exp(masked[u][n] - safe[u]).astype(jnp.bfloat16)
                grown = weight.astype(jnp.float32)
                sums[u] = grown if n == 0 else sums[u] + grown
                both.append(weight)
            vals = jnp.concatenate(
                [vbuf[2 * step, c:c + chunk, :], vbuf[2 * step + 1, c:c + chunk, :]], axis=1
            )
            values = values + jnp.dot(
                jnp.concatenate(both, axis=0), vals, preferred_element_type=jnp.float32
            )
        for u in range(2):
            s = 2 * pair + u
            fresh_weight = jnp.exp(fresh_scores[u] - safe[u]).astype(jnp.bfloat16)
            fresh_weight = fresh_weight.astype(jnp.float32)
            amount = jnp.sum(sums[u], axis=1, keepdims=True) + fresh_weight
            weighted = values[u * 2 * hh:(u + 1) * 2 * hh, u * LANES:(u + 1) * LANES]
            weighted = weighted + fresh_weight * fresh_values[u]
            mine[s, :2 * hh, :] = weighted
            mine[s, 2 * hh:, :] = jnp.where(wide < DH, tops[u], amount)
            owner, copy = send_partial(s)

            @pl.when(owner != me)
            def _():
                copy.start()

        return carry

    lax.fori_loop(0, npairs, attend, 0)

    gains = hg[...]
    row_h = lax.broadcasted_iota(jnp.int32, (hh, LANES), 0)
    lambda_rows = jnp.zeros((hh, LANES), jnp.float32)
    for h in range(hh):
        lambda_rows = jnp.where(row_h == h, lam_s[h], lambda_rows)
    for n in range(spk):
        s = me * spk + n
        blocks = [mine[s]]
        for j in range(1, n_kv):
            pltpu.make_async_remote_copy(
                mine.at[s], mine_in.at[j - 1, n], s3.at[s], r3.at[j - 1, n],
                device_id=kv_peer(j), device_id_type=MESH,
            ).wait_recv()
            blocks.append(mine_in[j - 1, n])
        maxima, amounts = [], []
        for piece in blocks:
            packed = piece[2 * hh:]
            swapped = pltpu.roll(packed, DH, 1)
            maxima.append(jnp.where(wide < DH, packed, swapped))
            amounts.append(jnp.where(wide < DH, swapped, packed))
        top = functools.reduce(jnp.maximum, maxima)
        amount = jnp.zeros_like(top)
        weighted = jnp.zeros_like(top)
        for piece, biggest, sum_there in zip(blocks, maxima, amounts):
            factor = jnp.exp(biggest - top)
            amount = amount + factor * sum_there
            weighted = weighted + factor * piece[:2 * hh]
        ratio = weighted / amount
        mixed = ratio[:hh] - lambda_rows * ratio[hh:]
        mean = jnp.mean(mixed * mixed, axis=1, keepdims=True)
        head_out = mixed * lax.rsqrt(mean + epsilon) * gains
        heads[pl.ds(pl.multiple_of(s * 2 * hh, 2 * hh), 2 * hh), :] = jnp.concatenate(
            [head_out, head_out], axis=0
        )
    size = spk * 2 * hh
    own_heads = pl.ds(pl.multiple_of(me * size, size), size)
    for j in range(1, n_kv):
        copy = pltpu.make_async_remote_copy(
            heads.at[own_heads], heads.at[own_heads], s4.at[j - 1], r4.at[j - 1],
            device_id=kv_peer(j), device_id_type=MESH,
        )
        copy.start()
        sends.append(copy)
    out_weight_in.wait()
    for j in range(1, n_kv):
        source = lax.rem(me + n_kv - j, n_kv)
        there = pl.ds(pl.multiple_of(source * size, size), size)
        pltpu.make_async_remote_copy(
            heads.at[there], heads.at[there], s4.at[j - 1], r4.at[j - 1],
            device_id=kv_peer(j), device_id_type=MESH,
        ).wait_recv()
    head_row = jnp.concatenate(
        [heads[pl.ds(h, seqs, stride=2 * hh), :] for h in range(hh)], axis=1
    ).astype(jnp.bfloat16)
    share = jnp.dot(head_row, owbuf[...], preferred_element_type=jnp.float32)
    shares[tp] = share.astype(jnp.bfloat16)
    for j in range(1, n_tp):
        copy = pltpu.make_async_remote_copy(
            shares.at[tp], shares.at[tp], s5.at[j - 1], r5.at[j - 1],
            device_id=tp_peer(j), device_id_type=MESH,
        )
        copy.start()
        sends.append(copy)
    for j in range(1, n_tp):
        source = lax.rem(tp + n_tp - j, n_tp)
        pltpu.make_async_remote_copy(
            shares.at[source], shares.at[source], s5.at[j - 1], r5.at[j - 1],
            device_id=tp_peer(j), device_id_type=MESH,
        ).wait_recv()
    result = shares[0].astype(jnp.float32)
    for n in range(1, n_tp):
        result = result + shares[n].astype(jnp.float32)
    out_ref[...] = result.astype(out_ref.dtype)

    for copy in sends:
        copy.wait_send()

    def drain(step, carry):
        s = lax.rem((me + 1) * spk + step, seqs)
        _, copy = send_partial(s)
        copy.wait_send()
        return carry

    lax.fori_loop(0, seqs - spk, drain, 0)


def solution(mesh):
    n_kv, n_tp = mesh.shape["kv"], mesh.shape["tp"]

    def local(
        tokens, norm_gain, query_weight, key_weight, value_weight, out_weight,
        lambdas, head_gain, lengths, key_cache, value_cache,
    ):
        seqs, width = tokens.shape
        inner = query_weight.shape[1]
        hh = inner // LANES
        out_width = out_weight.shape[1]
        cols = key_cache.shape[1] * hh
        spk = seqs // n_kv
        flat = (seqs, cols, LANES)
        halfway = DH // 2
        frequency = np.float32(theta_base) ** (
            -(np.arange(LANES) % halfway).astype(np.float64) / halfway
        )
        frequency = jnp.asarray(frequency.astype(np.float32)[None, :])
        whole = pl.BlockSpec(memory_space=pl.ANY)
        scalars = pl.BlockSpec(memory_space=pltpu.SMEM)
        dma = pltpu.SemaphoreType.DMA
        return pl.pallas_call(
            functools.partial(kernel, n_kv, n_tp),
            out_shape=jax.ShapeDtypeStruct((seqs, out_width), jnp.bfloat16),
            in_specs=[whole] * 6 + [scalars, whole, scalars] + [whole] * 3,
            out_specs=pl.BlockSpec(memory_space=pltpu.VMEM),
            scratch_shapes=[
                pltpu.VMEM((seqs, width), jnp.bfloat16),
                pltpu.VMEM((1, width), jnp.float32),
                pltpu.VMEM((3, width, inner), jnp.bfloat16),
                pltpu.VMEM((inner, out_width), jnp.bfloat16),
                pltpu.VMEM((1, LANES), jnp.float32),
                pltpu.VMEM((1, LANES), jnp.float32),
                pltpu.VMEM(flat, jnp.bfloat16),
                pltpu.VMEM(flat, jnp.bfloat16),
                pltpu.VMEM((2 * hh, cols), jnp.int32),
                pltpu.VMEM((seqs * ROWS, LANES), jnp.float32),
                pltpu.VMEM((n_kv - 1, spk * ROWS, LANES), jnp.float32),
                pltpu.VMEM((seqs * ROWS, LANES), jnp.bfloat16),
                pltpu.VMEM((seqs, 4 * hh, LANES), jnp.float32),
                pltpu.VMEM((n_kv - 1, spk, 4 * hh, LANES), jnp.float32),
                pltpu.VMEM((seqs * 2 * hh, LANES), jnp.float32),
                pltpu.VMEM((n_tp, seqs, out_width), jnp.bfloat16),
                dma((4,)), dma((4,)), dma((seqs // 2,)), dma((seqs // 2,)),
                dma((n_kv - 1,)), dma((n_kv - 1,)),
                dma((n_kv - 1,)), dma((n_kv - 1,)),
                dma((seqs,)), dma((n_kv - 1, spk)),
                dma((n_kv - 1,)), dma((n_kv - 1,)),
                dma((n_tp - 1,)), dma((n_tp - 1,)),
            ],
            compiler_params=pltpu.CompilerParams(
                collective_id=0, has_side_effects=True, vmem_limit_bytes=60 * 1024 * 1024
            ),
        )(
            tokens, norm_gain.reshape(1, width), query_weight, key_weight, value_weight,
            out_weight, lambdas, head_gain.reshape(1, LANES), lengths, frequency,
            key_cache.reshape(flat), value_cache.reshape(flat),
        )

    return jax.shard_map(
        local,
        mesh=mesh,
        in_specs=(
            P(None, "kv"), P("kv"), P("kv", "tp"), P("kv", "tp"), P("kv", "tp"), P("tp", "kv"),
            P("tp"), P(), P(), P(None, "kv", "tp", None), P(None, "kv", "tp", None),
        ),
        out_specs=P(None, "kv"),
        check_vma=False,
    )
```

time: 226 us -> 45.6 us (0.20)
  blocking collectives: 103 us -> 0 us
  waiting for transfers between devices: 44.7 us -> 0 us
  Pallas kernels: 0 us -> 44 us
  local copies, waits for them, and re-layouts: 30.3 us -> 1.32 us
  matrix products: 21.7 us -> 0 us
  between operations: 13.6 us -> 0.01 us
  other arithmetic: 11.1 us -> 0 us
    all_gather x3 -> x0, blocking collectives: 92.6 us -> none  [combined_all(): pieces = jax.tree.map(lambda part: lax.all_gather(part, axis), value)]
    psum x1 -> x0, waiting for transfers between devices: 44.6 us -> none  [local(): lax.psum((query_part, key_part, value_part, squares), 'kv')]
    pallas_call x0 -> x1, Pallas kernels: none -> 44 us  [local(): pl.pallas_call(functools.partial(kernel, n_kv, n_tp), out_shape=jax.Shape...]
    unnamed x7 -> x1, local copies, waits for them, and re-layouts: 26.2 us -> 1.32 us
    dot_general x6 -> x0, matrix products: 21.7 us -> none  [the longest x1 8.24 us: local(): jnp.einsum('shjp,sphe->shje', cached_weights, value_cache, preferred_elem...]
    psum x1 -> x0, blocking collectives: 10.9 us -> none  [local(): return lax.psum(partial_value, 'tp').astype(jnp.bfloat16)]
    reduce_sum x3 -> x0, other arithmetic: 3.33 us -> none  [the longest x1 1.68 us: local(): jnp.sum(jnp.where(at_length, weights, jnp.zeros_like(weights)).astype(jnp...]
    add x15 -> x0, other arithmetic: 3.19 us -> none  [the longest x7 2.97 us: combine(): former[2] * former_scale[..., None] + latter[2] * latter_scale[..., None]]
  transfers between devices with their start and end apart: 1 -> 0, of which waited for: 1 -> 0; matrix products, arithmetic and copies ran while one was open for 13% -> 0% of each run, Pallas kernels for 0% -> 0%
where the time goes in v1:
time: 45.6 us; the launch traced here: 45.4 us
  Pallas kernels  44 us (96%)
  local copies, waits for them, and re-layouts  1.32 us (3%)
    pallas_call x1, Pallas kernels, local(): pl.pallas_call(functools.partial(kernel, n_kv, n_tp), out_shape=jax.Shape...  44 us
    unnamed x1, local copies, waits for them, and re-layouts  1.32 us

profile of v1, /device:TPU:0, one launch (start us, length us, event | category | flops | bytes accessed | tf_op | source)
XLA Modules:
  0.0 45.4 jit_solution(8765638651586357675)
XLA Ops:
  0.0 44.0 %shard_map.118 = bf16[16,512]{1,0:T(8,128)(2,1)} custom-call(bf16[16,512]{1,0:T(8,128)(2,1)} %tok_h.1, f32[1,512]{1,0:T(1,128)} %bitcast.6, bf16[512,512]{1,0:T(8,128)(2,1)} %qw_h.1, bf16[512,512]{1,0:T(8,128)(2,1)} %kw_h.1, bf16[512,512]{1,0:T(8,128)(2,1)} %vw_h.1, bf16[512,512]{1,0:T(8,128)(2,1)} %ow_h.1, f32[4]{0:T(128)} %lam_s.1, f32[1,128]{1,0:T(1,128)} %bitcast.7, ...), custom_call_target="tpu_custom_call" | custom-call | tf_op jit(solution)/shard_map/pallas_call | solution.py:361
  44.0 1.3 %copy.14 = bf16[16,512]{1,0:T(8,128)(2,1)} copy(bf16[16,512]{1,0:T(8,128)(2,1)} %shard_map.118) | data formatting | bytes 32768

commit v2 on v1

--- a/solution.py
+++ b/solution.py
@@ -40,6 +40,18 @@
     base = me * pos_count
     start_pair = lax.div((me + 1) * spk + 1, 2)
 
+    def kv_peer(j):
+        return {"kv": lax.rem(me + j, n_kv), "tp": tp}
+
+    def tp_peer(j):
+        return {"kv": me, "tp": lax.rem(tp + j, n_tp)}
+
+    barrier = pltpu.get_barrier_semaphore()
+    for j in range(1, n_kv):
+        pl.semaphore_signal(barrier, inc=1, device_id=kv_peer(j), device_id_type=MESH)
+    for j in range(1, n_tp):
+        pl.semaphore_signal(barrier, inc=1, device_id=tp_peer(j), device_id_type=MESH)
+
     small = [
         pltpu.make_async_copy(src, dst, small_sem.at[n])
         for n, (src, dst) in enumerate(((tok_h, tok), (gain_h, gain), (freq_h, freq), (hg_h, hg)))
@@ -62,23 +74,6 @@
             pltpu.make_async_copy(v_h.at[at], vbuf.at[pl.ds(2 * step, 2)], v_sem.at[step]),
         )
 
-    for step in range(npairs):
-        for copy in cache_copies(step):
-            copy.start()
-        if step == npairs // 2:
-            out_weight_in.start()
-
-    def kv_peer(j):
-        return {"kv": lax.rem(me + j, n_kv), "tp": tp}
-
-    def tp_peer(j):
-        return {"kv": me, "tp": lax.rem(tp + j, n_tp)}
-
-    barrier = pltpu.get_barrier_semaphore()
-    for j in range(1, n_kv):
-        pl.semaphore_signal(barrier, inc=1, device_id=kv_peer(j), device_id_type=MESH)
-    for j in range(1, n_tp):
-        pl.semaphore_signal(barrier, inc=1, device_id=tp_peer(j), device_id_type=MESH)
 
     column = lax.broadcasted_iota(jnp.int32, (2 * hh, cols), 1)
     row = lax.broadcasted_iota(jnp.int32, (2 * hh, cols), 0)
@@ -106,6 +101,11 @@
         for h in range(hh):
             part[pl.ds(n * hh + h, seqs, stride=ROWS), :] = product[:, h * LANES:(h + 1) * LANES]
 
+    for step in range(npairs):
+        for copy in cache_copies(step):
+            copy.start()
+        if step == npairs // 2:
+            out_weight_in.start()
     pl.semaphore_wait(barrier, n_kv - 1 + n_tp - 1)
 
     block = spk * ROWS

time: 45.6 us -> 39.2 us (0.86)
  Pallas kernels: 44 us -> 37.5 us
    pallas_call x1, Pallas kernels: 44 us -> 37.5 us  [local(): pl.pallas_call(functools.partial(kernel, n_kv, n_tp), out_shape=jax.Shape...]
where the time goes in v2:
time: 39.2 us; the launch traced here: 38.8 us
  Pallas kernels  37.5 us (96%)
  local copies, waits for them, and re-layouts  1.32 us (3%)
    pallas_call x1, Pallas kernels, local(): pl.pallas_call(functools.partial(kernel, n_kv, n_tp), out_shape=jax.Shape...  37.5 us
    unnamed x1, local copies, waits for them, and re-layouts  1.32 us

profile of v2, /device:TPU:0, one launch (start us, length us, event | category | flops | bytes accessed | tf_op | source)
XLA Modules:
  0.0 38.8 jit_solution(2864728114145166606)
XLA Ops:
  0.0 37.5 %shard_map.118 = bf16[16,512]{1,0:T(8,128)(2,1)} custom-call(bf16[16,512]{1,0:T(8,128)(2,1)} %tok_h.1, f32[1,512]{1,0:T(1,128)} %bitcast.6, bf16[512,512]{1,0:T(8,128)(2,1)} %qw_h.1, bf16[512,512]{1,0:T(8,128)(2,1)} %kw_h.1, bf16[512,512]{1,0:T(8,128)(2,1)} %vw_h.1, bf16[512,512]{1,0:T(8,128)(2,1)} %ow_h.1, f32[4]{0:T(128)} %lam_s.1, f32[1,128]{1,0:T(1,128)} %bitcast.7, ...), custom_call_target="tpu_custom_call" | custom-call | tf_op jit(solution)/shard_map/pallas_call | solution.py:361
  37.5 1.3 %copy.14 = bf16[16,512]{1,0:T(8,128)(2,1)} copy(bf16[16,512]{1,0:T(8,128)(2,1)} %shard_map.118) | data formatting | bytes 32768
